TPU v7x, 512 devices: a whole 4x4x16 slice. The times are simulated.
512 devices in a mesh: rep: 2 (over z_hi), fs: 32 (over z_lo, y), tp: 8 (over x, core).
Axes of the slice: x: 4, y: 4, z: 16 (z_hi: 2, z_lo: 8; z = z_hi * 8 + z_lo), core: 2. Of those that a mesh axis runs over, the one named last changes fastest.
Arguments:
- stream: bfloat16 [16384, 2048], P(('rep', 'fs'), 'tp'), may hold values from -6 to 6
- norm_gains: float32 [6, 2048], replicated, may hold values from 0.1 to 1.9
- w_gate: bfloat16 [2048, 5632], P('fs', 'tp'), may hold values from -0.125 to 0.125
- w_up: bfloat16 [2048, 5632], P('fs', 'tp'), may hold values from -0.125 to 0.125
- w_down: bfloat16 [5632, 2048], P('tp', 'fs'), may hold values from -0.15625 to 0.15625
- w_inner: bfloat16 [2048, 1024], P('fs', 'tp'), may hold values from -0.125 to 0.125
- w_bgate: bfloat16 [2048, 1024], P('fs', 'tp'), may hold values from -0.125 to 0.125
- w_cgate: bfloat16 [2048, 1024], P('fs', 'tp'), may hold values from -0.125 to 0.125
- conv_taps: float32 [3, 1024], P(None, 'tp'), may hold values from -3.5 to 3.5
- w_out: bfloat16 [1024, 2048], P('tp', 'fs'), may hold values from -0.375 to 0.375
Outputs:
- mixed: bfloat16 [16384, 2048], P(('rep', 'fs'), 'tp')
All inputs are finite; a program needn't handle non-finite values.
Results may differ from a plain program's by a relative error of at most 0.02.
Values may be sent and summed in bfloat16 or wider, within the bound.
A program may use at most 64 MiB of HBM per device.

v0:
```python
import jax
import jax.numpy as jnp
from jax import lax
from jax.sharding import PartitionSpec as P

TAPS = 3
EPSILON = 1e-06


def laid_out(parts, dim):
    shape = list(parts.shape[1:])
    shape[dim] *= parts.shape[0]
    return jnp.moveaxis(parts, 0, dim).reshape(shape)


def from_everyone(x, axis):
    copies = jnp.broadcast_to(x, (lax.axis_size(axis), *x.shape))
    return lax.all_to_all(copies, axis, split_axis=0, concat_axis=0, tiled=True)


def collect(x, axis, dim):
    return laid_out(from_everyone(x, axis), dim)


def cut_along(x, dim, count):
    shape = x.shape
    parts = x.reshape(*shape[:dim], count, shape[dim] // count, *shape[dim + 1 :])
    return jnp.moveaxis(parts, dim, 0)


def sent_and_summed(x, axis, dim):
    parts = cut_along(x, dim, lax.axis_size(axis))
    arrived = lax.all_to_all(parts, axis, split_axis=0, concat_axis=0, tiled=True)
    return arrived.astype(jnp.float32).sum(axis=0)


def taken_together(x, axis):
    everything = from_everyone(x, axis)
    return jnp.sum(everything, axis=0)


def rows_first(arrays, axis, dims):
    turned = [jnp.moveaxis(a, dim, 0) for a, dim in zip(arrays, dims)]
    both = jnp.concatenate([t.reshape(len(t), -1) for t in turned], axis=1)
    whole, at, done = (lax.all_gather(both, axis, axis=0, tiled=True), 0, [])
    for t, dim in zip(turned, dims):
        slab = whole[:, at : at + t[0].size].reshape(-1, *t.shape[1:])
        done.append(jnp.moveaxis(slab, 0, dim))
        at += t[0].size
    return tuple(done)


def from_behind(x, axis, by):
    count = lax.axis_size(axis)
    pairs = [(i, i + by) for i in range(count) if 0 <= i + by < count]
    return lax.ppermute(x, axis, pairs)


def shards(stream, norm_gains, w_gate, w_up, w_down, w_inner, w_bgate, w_cgate, conv_taps, w_out):
    tp_index = lax.axis_index("tp")
    local_width = stream.shape[1]
    model_width = local_width * lax.axis_size("tp")

    def own_gain(row):
        return lax.dynamic_slice_in_dim(norm_gains[row], tp_index * local_width, local_width, 0)

    def gathered_norm(current, row):
        gathered = collect(current, "tp", 1)
        values = gathered.astype(jnp.float32)
        scaled = values * lax.rsqrt(jnp.mean(values * values, axis=1, keepdims=True) + EPSILON)
        return (scaled * norm_gains[row]).astype(jnp.bfloat16)

    def settle(current, partials, row, weight):
        branch_sum = sent_and_summed(partials.astype(jnp.bfloat16), "tp", 1)
        squares = taken_together(jnp.sum(branch_sum * branch_sum, axis=1), "tp")
        scaled = branch_sum * lax.rsqrt(squares / model_width + EPSILON)[:, None]
        return (current.astype(jnp.float32) + weight * (scaled * own_gain(row))).astype(
            jnp.bfloat16
        )

    gate_whole, up_whole, down_whole = rows_first((w_gate, w_up, w_down), "fs", (0, 0, 1))

    def feed_forward(current, row_in, row_out):
        normed = gathered_norm(current, row_in)
        gate_vals = jnp.dot(normed, gate_whole, preferred_element_type=jnp.float32)
        upward = jnp.dot(normed, up_whole, preferred_element_type=jnp.float32)
        hidden = (jax.nn.silu(gate_vals) * upward).astype(jnp.bfloat16)
        partials = jnp.dot(hidden, down_whole, preferred_element_type=jnp.float32)
        return settle(current, partials, row_out, 0.5)

    first = feed_forward(stream, 0, 1)
    normed_mix = gathered_norm(first, 2)
    local_rows = normed_mix.shape[0]

    def fold_rows(block_rows):
        return jnp.dot(normed_mix, block_rows, preferred_element_type=jnp.float32)

    inner = fold_rows(collect(w_inner, "fs", 0))
    bgate = fold_rows(collect(w_bgate, "fs", 0))
    cgate = fold_rows(collect(w_cgate, "fs", 0))
    conv_input = cgate * inner
    earlier = from_behind(conv_input[local_rows - (TAPS - 1) :], "fs", 1)
    padded = jnp.concatenate([earlier, conv_input], axis=0)
    conv = conv_taps[0] * padded[0:local_rows]
    for tap in range(1, TAPS):
        conv = conv + conv_taps[tap] * padded[tap : tap + local_rows]
    gated = (bgate * conv).astype(jnp.bfloat16)
    mix_partials = jnp.dot(gated, collect(w_out, "fs", 1), preferred_element_type=jnp.float32)
    second = settle(first, mix_partials, 3, 1.0)
    return feed_forward(second, 4, 5)


def solution(mesh):
    return jax.shard_map(
        shards,
        mesh=mesh,
        in_specs=(
            P(("rep", "fs"), "tp"),
            P(),
            P("fs", "tp"),
            P("fs", "tp"),
            P("tp", "fs"),
            P("fs", "tp"),
            P("fs", "tp"),
            P("fs", "tp"),
            P(None, "tp"),
            P("tp", "fs"),
        ),
        out_specs=P(("rep", "fs"), "tp"),
        check_vma=False,
    )
```

profile of v0, /device:TPU:1, one launch (start us, length us, event | category | flops | bytes accessed | tf_op | source)
XLA Modules:
  0.0 521.1 jit_solution(112186578533772279)
XLA Ops:
  9.5 24.3 %all_to_all.68 = bf16[8,256,256]{1,2,0:T(8,128)(2,1)S(1)} all-to-all(bf16[8,256,256]{1,2,0:T(8,128)(2,1)S(1)} %broadcast_in_dim.39), channel_id=1, replica_groups=mesh['rep'=2,'fs'=32,'tp'=8] {'tp'}, dimensions={0} | all-to-all | bytes 2097152 | tf_op jit(solution)/shard_map/all_to_all | solution.py:18
  34.8 11.8 %all-to-all-start.5 = ((bf16[32,64,128]{2,1,0:T(8,128)(2,1)}), bf16[32,64,128]{2,1,0:T(8,128)(2,1)S(1)}, u32[]{:S(2)}, u32[]{:S(2)}) async-start(bf16[32,64,128]{2,1,0:T(8,128)(2,1)} %broadcast_in_dim.43), calls=%async_computation.5 | async-start | bytes 1048576 | tf_op jit(solution)/shard_map/all_to_all | solution.py:18
  48.0 186.2 %all-gather.2.cloned.1.call-done = bf16[2048,2112]{1,0:T(8,128)(2,1)} async-done(((bf16[64,2112]{1,0:T(8,128)(2,1)}), bf16[2048,2112]{1,0:T(8,128)(2,1)}) %all-gather.2.cloned.1.call-update) | async-done | bytes 8650768 | tf_op jit(solution)/shard_map/all_gather | solution.py:45
  234.2 3.2 fusion.10
  237.4 7.4 %fusion.12 = bf16[256,2048]{1,0:T(8,128)(2,1)S(1)} fusion(bf16[2048,2112]{1,0:T(8,128)(2,1)} %all-gather.2.cloned.1.call-done, bf16[256,2048]{0,1:T(8,128)(2,1)S(1)} %fusion.24, f32[256,704]{0,1:T(8,128)S(1)} %fusion.10), kind=kOutput, calls=%fused_computation.15 | convolution fusion | flops 1478000640 | bytes 9109504 | tf_op jit(solution)/shard_map/dot_general | solution.py:88
  245.8 41.3 %all_to_all.69 = bf16[8,256,256]{2,1,0:T(8,128)(2,1)S(1)} all-to-all(bf16[8,256,256]{2,1,0:T(8,128)(2,1)S(1)} %bitcast.73), channel_id=1, replica_groups=mesh['rep'=2,'fs'=32,'tp'=8] {'tp'}, dimensions={0} | all-to-all | bytes 2097152 | tf_op jit(solution)/shard_map/all_to_all | solution.py:33
  288.0 8.5 %all-to-all-start.6 = ((bf16[32,64,128]{2,1,0:T(8,128)(2,1)}), bf16[32,64,128]{2,1,0:T(8,128)(2,1)S(1)}, u32[]{:S(2)}, u32[]{:S(2)}) async-start(bf16[32,64,128]{2,1,0:T(8,128)(2,1)} %broadcast_in_dim.44), calls=%async_computation.6 | async-start | bytes 1048576 | tf_op jit(solution)/shard_map/all_to_all | solution.py:18
  296.8 26.5 %all-to-all-done.6 = bf16[32,64,128]{2,1,0:T(8,128)(2,1)S(1)} async-done(((bf16[32,64,128]{2,1,0:T(8,128)(2,1)}), bf16[32,64,128]{2,1,0:T(8,128)(2,1)S(1)}, u32[]{:S(2)}, u32[]{:S(2)}) %all-to-all-start.6) | async-done | bytes 524320 | tf_op jit(solution)/shard_map/all_to_all | solution.py:18
  323.3 10.8 %all_to_all.70 = f32[8,1,256]{2,1,0:T(1,128)S(1)} all-to-all(f32[8,1,256]{2,1,0:T(1,128)S(1)} %broadcast_in_dim.40), channel_id=1, replica_groups=mesh['rep'=2,'fs'=32,'tp'=8] {'tp'}, dimensions={0} | all-to-all | bytes 16384 | tf_op jit(solution)/shard_map/all_to_all | solution.py:18
  335.0 5.8 %all-to-all-start.7 = ((bf16[32,128,64]{1,2,0:T(8,128)(2,1)}), bf16[32,128,64]{1,2,0:T(8,128)(2,1)S(1)}, u32[]{:S(2)}, u32[]{:S(2)}) async-start(bf16[32,128,64]{1,2,0:T(8,128)(2,1)} %broadcast_in_dim.45), calls=%async_computation.7 | async-start | bytes 1048576 | tf_op jit(solution)/shard_map/all_to_all | solution.py:18
  341.7 25.8 %all-to-all-done.7 = bf16[32,128,64]{1,2,0:T(8,128)(2,1)S(1)} async-done(((bf16[32,128,64]{1,2,0:T(8,128)(2,1)}), bf16[32,128,64]{1,2,0:T(8,128)(2,1)S(1)}, u32[]{:S(2)}, u32[]{:S(2)}) %all-to-all-start.7) | async-done | bytes 524320 | tf_op jit(solution)/shard_map/all_to_all | solution.py:18
  367.6 21.2 %all_to_all.71 = bf16[8,256,256]{1,2,0:T(8,128)(2,1)S(1)} all-to-all(bf16[8,256,256]{1,2,0:T(8,128)(2,1)S(1)} %broadcast_in_dim.41), channel_id=1, replica_groups=mesh['rep'=2,'fs'=32,'tp'=8] {'tp'}, dimensions={0} | all-to-all | bytes 2097152 | tf_op jit(solution)/shard_map/all_to_all | solution.py:18
  389.7 5.9 %all-to-all-start.4 = ((bf16[32,64,128]{2,1,0:T(8,128)(2,1)}), bf16[32,64,128]{2,1,0:T(8,128)(2,1)}, u32[]{:S(2)}, u32[]{:S(2)}) async-start(bf16[32,64,128]{2,1,0:T(8,128)(2,1)} %broadcast_in_dim.42), calls=%async_computation.4 | async-start | bytes 1048576 | tf_op jit(solution)/shard_map/all_to_all | solution.py:18
  398.4 3.1 collective-permute-start
  401.5 20.9 %all-to-all-done.4 = bf16[32,64,128]{2,1,0:T(8,128)(2,1)} async-done(((bf16[32,64,128]{2,1,0:T(8,128)(2,1)}), bf16[32,64,128]{2,1,0:T(8,128)(2,1)}, u32[]{:S(2)}, u32[]{:S(2)}) %all-to-all-start.4) | async-done | bytes 524320 | tf_op jit(solution)/shard_map/all_to_all | solution.py:18
  424.4 21.4 %all_to_all.72 = bf16[8,256,256]{2,1,0:T(8,128)(2,1)S(1)} all-to-all(bf16[8,256,256]{2,1,0:T(8,128)(2,1)S(1)} %bitcast.74), channel_id=1, replica_groups=mesh['rep'=2,'fs'=32,'tp'=8] {'tp'}, dimensions={0} | all-to-all | bytes 2097152 | tf_op jit(solution)/shard_map/all_to_all | solution.py:33
  446.6 4.3 all-to-all-start.9
  451.5 4.0 all-to-all-done.9
  455.8 18.1 %all_to_all.73 = bf16[8,256,256]{1,2,0:T(8,128)(2,1)S(1)} all-to-all(bf16[8,256,256]{1,2,0:T(8,128)(2,1)S(1)} %broadcast_in_dim.47), channel_id=1, replica_groups=mesh['rep'=2,'fs'=32,'tp'=8] {'tp'}, dimensions={0} | all-to-all | bytes 2097152 | tf_op jit(solution)/shard_map/all_to_all | solution.py:18
  474.5 3.2 fusion.8
  477.7 7.4 %fusion.15 = bf16[256,2048]{1,0:T(8,128)(2,1)S(1)} fusion(bf16[2048,2112]{1,0:T(8,128)(2,1)} %all-gather.2.cloned.1.call-done, bf16[256,2048]{0,1:T(8,128)(2,1)S(1)} %fusion.22, f32[256,704]{0,1:T(8,128)S(1)} %fusion.8), kind=kOutput, calls=%fused_computation.16 | convolution fusion | flops 1478000640 | bytes 9109504 | tf_op jit(solution)/shard_map/dot_general | solution.py:88
  485.2 18.4 %all_to_all.74 = bf16[8,256,256]{2,1,0:T(8,128)(2,1)S(1)} all-to-all(bf16[8,256,256]{2,1,0:T(8,128)(2,1)S(1)} %bitcast.75), channel_id=1, replica_groups=mesh['rep'=2,'fs'=32,'tp'=8] {'tp'}, dimensions={0} | all-to-all | bytes 2097152 | tf_op jit(solution)/shard_map/all_to_all | solution.py:33
  504.5 4.3 all-to-all-start.12
  509.4 4.0 all-to-all-done.12
  (71 shorter events, 19.6 us)
Async XLA Ops:
  6.5 227.7 %all-gather.2.cloned.1.call-start = ((), (), s32[]{:S(2)}) async-start(), calls=%async_computation.13 | async-start | bytes 9191424 | tf_op jit(solution)/shard_map/all_gather | solution.py:45
  6.5 27.3 %copy-start.3 = (bf16[64,128]{1,0:T(8,128)(2,1)S(1)}, bf16[64,128]{1,0:T(8,128)(2,1)}, u32[]{:S(2)}) copy-start(bf16[64,128]{1,0:T(8,128)(2,1)} %param.17) | copy-start | bytes 49156
  9.5 37.2 %copy-start.2 = (f32[6,2048]{1,0:T(8,128)S(1)}, f32[6,2048]{1,0:T(8,128)}, u32[]{:S(2)}) copy-start(f32[6,2048]{1,0:T(8,128)} %param.11) | copy-start | bytes 147460
  34.8 210.1 %all-to-all-start.5 = ((bf16[32,64,128]{2,1,0:T(8,128)(2,1)}), bf16[32,64,128]{2,1,0:T(8,128)(2,1)S(1)}, u32[]{:S(2)}, u32[]{:S(2)}) async-start(bf16[32,64,128]{2,1,0:T(8,128)(2,1)} %broadcast_in_dim.43), calls=%async_computation.5 | async-start | bytes 1048576 | tf_op jit(solution)/shard_map/all_to_all | solution.py:18
  244.9 42.2 %copy-start.4 = (bf16[64,128]{1,0:T(8,128)(2,1)S(1)}, bf16[64,128]{1,0:T(8,128)(2,1)}, u32[]{:S(2)}) copy-start(bf16[64,128]{1,0:T(8,128)(2,1)} %param.15) | copy-start | bytes 49156
  244.9 0.9 copy-start
  287.1 47.0 %copy-start.5 = (bf16[128,64]{0,1:T(8,128)(2,1)S(1)}, bf16[128,64]{0,1:T(8,128)(2,1)}, u32[]{:S(2)}) copy-start(bf16[128,64]{0,1:T(8,128)(2,1)} %param.19) | copy-start | bytes 49156
  288.0 53.5 %copy-start.1 = (bf16[256,256]{1,0:T(8,128)(2,1)S(1)}, bf16[256,256]{1,0:T(8,128)(2,1)}, u32[]{:S(2)}) copy-start(bf16[256,256]{1,0:T(8,128)(2,1)} %param.10) | copy-start | bytes 393220
  288.0 35.3 %all-to-all-start.6 = ((bf16[32,64,128]{2,1,0:T(8,128)(2,1)}), bf16[32,64,128]{2,1,0:T(8,128)(2,1)S(1)}, u32[]{:S(2)}, u32[]{:S(2)}) async-start(bf16[32,64,128]{2,1,0:T(8,128)(2,1)} %broadcast_in_dim.44), calls=%async_computation.6 | async-start | bytes 1048576 | tf_op jit(solution)/shard_map/all_to_all | solution.py:18
  335.0 32.6 %all-to-all-start.7 = ((bf16[32,128,64]{1,2,0:T(8,128)(2,1)}), bf16[32,128,64]{1,2,0:T(8,128)(2,1)S(1)}, u32[]{:S(2)}, u32[]{:S(2)}) async-start(bf16[32,128,64]{1,2,0:T(8,128)(2,1)} %broadcast_in_dim.45), calls=%async_computation.7 | async-start | bytes 1048576 | tf_op jit(solution)/shard_map/all_to_all | solution.py:18
  340.8 48.0 %copy-start.6 = (bf16[64,128]{1,0:T(8,128)(2,1)S(1)}, bf16[64,128]{1,0:T(8,128)(2,1)}, u32[]{:S(2)}) copy-start(bf16[64,128]{1,0:T(8,128)(2,1)} %param.16) | copy-start | bytes 49156
  389.7 32.7 %all-to-all-start.4 = ((bf16[32,64,128]{2,1,0:T(8,128)(2,1)}), bf16[32,64,128]{2,1,0:T(8,128)(2,1)}, u32[]{:S(2)}, u32[]{:S(2)}) async-start(bf16[32,64,128]{2,1,0:T(8,128)(2,1)} %broadcast_in_dim.42), calls=%async_computation.4 | async-start | bytes 1048576 | tf_op jit(solution)/shard_map/all_to_all | solution.py:18
  396.4 5.1 copy-start.7
  398.4 24.0 %collective-permute-start = (f32[2,128]{1,0:T(2,128)S(1)}, f32[2,128]{1,0:T(2,128)S(1)}, u32[]{:S(2)}, u32[]{:S(2)}) collective-permute-start(f32[2,128]{1,0:T(2,128)S(1)} %slice.63), channel_id=1, source_target_pairs={{0,8},{8,16},{16,24},{24,32},{32,40},{40,48},{48,56},{56,64},{64,7... | collective-permute-start | bytes 3080 | tf_op jit(solution)/shard_map/ppermute | solution.py:56
  446.6 8.9 %all-to-all-start.9 = ((f32[8,1,256]{2,1,0:T(1,128)}), f32[8,1,256]{2,1,0:T(1,128)S(1)}, u32[]{:S(2)}, u32[]{:S(2)}) async-start(f32[8,1,256]{2,1,0:T(1,128)} %broadcast_in_dim.46), calls=%async_computation.9 | async-start | bytes 16384 | tf_op jit(solution)/shard_map/all_to_all | solution.py:18
  504.5 8.9 %all-to-all-start.12 = ((f32[8,1,256]{2,1,0:T(1,128)}), f32[8,1,256]{2,1,0:T(1,128)S(1)}, u32[]{:S(2)}, u32[]{:S(2)}) async-start(f32[8,1,256]{2,1,0:T(1,128)} %broadcast_in_dim.48), calls=%async_computation.12 | async-start | bytes 16384 | tf_op jit(solution)/shard_map/all_to_all | solution.py:18
Sparse Core Ops, SparseCore 0:
  9.4 224.7 all-gather.1
where the time goes:
time: 522 us; the launch traced here: 521 us
  waiting for transfers between devices  267 us (51%)
  blocking collectives  155 us (30%)
  starting transfers between devices  43.7 us (8%)
  matrix products  25 us (5%)
  between operations  13.7 us (3%)
  local copies, waits for them, and re-layouts  11.8 us (2%)
    all_gather x1, waiting for transfers between devices, rows_first(): whole, at, done = (lax.all_gather(both, axis, axis=0, tiled=True), 0, [])  186 us
    all_to_all x6, waiting for transfers between devices, from_everyone(): return lax.all_to_all(copies, axis, split_axis=0, concat_axis=0, tiled=True)  81.2 us
    all_to_all x3, blocking collectives, sent_and_summed(): lax.all_to_all(parts, axis, split_axis=0, concat_axis=0, tiled=True)  81.1 us
    all_to_all x4, blocking collectives, from_everyone(): return lax.all_to_all(copies, axis, split_axis=0, concat_axis=0, tiled=True)  74.4 us
    all_to_all x6, starting transfers between devices, from_everyone(): return lax.all_to_all(copies, axis, split_axis=0, concat_axis=0, tiled=True)  40.6 us
    dot_general x2, matrix products, feed_forward(): partials = jnp.dot(hidden, down_whole, preferred_element_type=jnp.float32)  14.8 us
  transfers between devices with their start and end apart: 8, of which 6 were waited for; matrix products, arithmetic and copies ran while one was open for 4% of the time, Pallas kernels for 0%

commit v1 on v0

--- a/solution.py
+++ b/solution.py
@@ -5,6 +5,11 @@
 
 TAPS = 3
 EPSILON = 1e-06
+
+
+def all_by_exchange(x, mesh_axis, dim):
+    sent = jnp.stack([x] * lax.axis_size(mesh_axis))
+    return jnp.concatenate(lax.all_to_all(sent, mesh_axis, 0, 0), axis=dim)
 
 
 def laid_out(parts, dim):
@@ -42,7 +47,7 @@
 def rows_first(arrays, axis, dims):
     turned = [jnp.moveaxis(a, dim, 0) for a, dim in zip(arrays, dims)]
     both = jnp.concatenate([t.reshape(len(t), -1) for t in turned], axis=1)
-    whole, at, done = (lax.all_gather(both, axis, axis=0, tiled=True), 0, [])
+    whole, at, done = (all_by_exchange(both, axis, 0), 0, [])
     for t, dim in zip(turned, dims):
         slab = whole[:, at : at + t[0].size].reshape(-1, *t.shape[1:])
         done.append(jnp.moveaxis(slab, 0, dim))

time: 522 us -> 709 us (1.36)
  blocking collectives: 155 us -> 510 us
  waiting for transfers between devices: 267 us -> 113 us
  between operations: 13.7 us -> 0.36 us
    all_to_all x0 -> x1, blocking collectives: none -> 399 us  [all_by_exchange(): return jnp.concatenate(lax.all_to_all(sent, mesh_axis, 0, 0), axis=dim)]
    all_gather x1 -> x0, waiting for transfers between devices: 186 us -> none  [rows_first(): whole, at, done = (lax.all_gather(both, axis, axis=0, tiled=True), 0, [])]
    all_to_all x6 -> x7, waiting for transfers between devices: 81.2 us -> 113 us  [from_everyone(): return lax.all_to_all(copies, axis, split_axis=0, concat_axis=0, tiled=True)]
    all_to_all x4 -> x3, blocking collectives: 74.4 us -> 50.1 us  [from_everyone(): return lax.all_to_all(copies, axis, split_axis=0, concat_axis=0, tiled=True)]
    all_to_all x3, blocking collectives: 81.1 us -> 60.8 us  [sent_and_summed(): lax.all_to_all(parts, axis, split_axis=0, concat_axis=0, tiled=True)]
    all_to_all x6 -> x7, starting transfers between devices: 40.6 us -> 43.7 us  [from_everyone(): return lax.all_to_all(copies, axis, split_axis=0, concat_axis=0, tiled=True)]
  transfers between devices with their start and end apart: 8 -> 8, of which waited for: 6 -> 7; matrix products, arithmetic and copies ran while one was open for 4% -> 2% of each run, Pallas kernels for 0% -> 0%
where the time goes in v1:
time: 709 us; the launch traced here: 708 us
  blocking collectives  510 us (72%)
  waiting for transfers between devices  113 us (16%)
  starting transfers between devices  46.6 us (7%)
  matrix products  25 us (4%)
  local copies, waits for them, and re-layouts  9.1 us (1%)
    all_to_all x1, blocking collectives, all_by_exchange(): return jnp.concatenate(lax.all_to_all(sent, mesh_axis, 0, 0), axis=dim)  399 us
    all_to_all x7, waiting for transfers between devices, from_everyone(): return lax.all_to_all(copies, axis, split_axis=0, concat_axis=0, tiled=True)  113 us
    all_to_all x3, blocking collectives, sent_and_summed(): lax.all_to_all(parts, axis, split_axis=0, concat_axis=0, tiled=True)  60.8 us
    all_to_all x3, blocking collectives, from_everyone(): return lax.all_to_all(copies, axis, split_axis=0, concat_axis=0, tiled=True)  50.1 us
    all_to_all x7, starting transfers between devices, from_everyone(): return lax.all_to_all(copies, axis, split_axis=0, concat_axis=0, tiled=True)  43.7 us
    dot_general x2, matrix products, feed_forward(): partials = jnp.dot(hidden, down_whole, preferred_element_type=jnp.float32)  14.8 us
  transfers between devices with their start and end apart: 8, of which 7 were waited for; matrix products, arithmetic and copies ran while one was open for 2% of the time, Pallas kernels for 0%

profile of v1, /device:TPU:1, one launch (start us, length us, event | category | flops | bytes accessed | tf_op | source)
XLA Modules:
  0.0 708.0 jit_solution(3756277491699097522)
XLA Ops:
  2.1 10.3 %all-to-all-start = ((bf16[8,256,256]{1,2,0:T(8,128)(2,1)}), bf16[8,256,256]{1,2,0:T(8,128)(2,1)S(1)}, u32[]{:S(2)}, u32[]{:S(2)}) async-start(bf16[8,256,256]{1,2,0:T(8,128)(2,1)} %broadcast_in_dim.39), calls=%async_computation | async-start | bytes 2097152 | tf_op jit(solution)/shard_map/all_to_all | solution.py:23
  12.6 14.8 %all-to-all-done = bf16[8,256,256]{1,2,0:T(8,128)(2,1)S(1)} async-done(((bf16[8,256,256]{1,2,0:T(8,128)(2,1)}), bf16[8,256,256]{1,2,0:T(8,128)(2,1)S(1)}, u32[]{:S(2)}, u32[]{:S(2)}) %all-to-all-start) | async-done | bytes 1048608 | tf_op jit(solution)/shard_map/all_to_all | solution.py:23
  28.6 399.0 %all_to_all.73 = bf16[32,64,2112]{2,1,0:T(8,128)(2,1)} all-to-all(bf16[32,64,2112]{2,1,0:T(8,128)(2,1)S(1)} %stack.2), channel_id=1, replica_groups=mesh['rep'=2,'fs'=32,'tp'=8] {'fs'}, dimensions={0} | all-to-all | bytes 17301504 | tf_op jit(solution)/shard_map/all_to_all | solution.py:12
  428.6 7.0 all-to-all-start.8
  439.5 7.4 %fusion.12 = bf16[256,2048]{1,0:T(8,128)(2,1)S(1)} fusion(bf16[2048,2112]{1,0:T(8,128)(2,1)} %bitcast.74, bf16[256,2048]{0,1:T(8,128)(2,1)S(1)} %fusion.24, f32[256,704]{0,1:T(8,128)S(1)} %fusion.10), kind=kOutput, calls=%fused_computation.15 | convolution fusion | flops 1478000640 | bytes 9109504 | tf_op jit(solution)/shard_map/dot_general | solution.py:93
  447.0 15.3 %all-to-all-done.8 = bf16[32,128,64]{1,2,0:T(8,128)(2,1)S(1)} async-done(((bf16[32,128,64]{1,2,0:T(8,128)(2,1)}), bf16[32,128,64]{1,2,0:T(8,128)(2,1)S(1)}, u32[]{:S(2)}, u32[]{:S(2)}) %all-to-all-start.8) | async-done | bytes 524320 | tf_op jit(solution)/shard_map/all_to_all | solution.py:23
  462.4 21.2 %all_to_all.74 = bf16[8,256,256]{2,1,0:T(8,128)(2,1)S(1)} all-to-all(bf16[8,256,256]{2,1,0:T(8,128)(2,1)S(1)} %bitcast.78), channel_id=1, replica_groups=mesh['rep'=2,'fs'=32,'tp'=8] {'tp'}, dimensions={0} | all-to-all | bytes 2097152 | tf_op jit(solution)/shard_map/all_to_all | solution.py:38
  484.5 5.9 all-to-all-start.6
  490.7 26.5 %all-to-all-done.6 = bf16[32,64,128]{2,1,0:T(8,128)(2,1)S(1)} async-done(((bf16[32,64,128]{2,1,0:T(8,128)(2,1)}), bf16[32,64,128]{2,1,0:T(8,128)(2,1)S(1)}, u32[]{:S(2)}, u32[]{:S(2)}) %all-to-all-start.6) | async-done | bytes 524320 | tf_op jit(solution)/shard_map/all_to_all | solution.py:23
  517.2 10.8 %all_to_all.75 = f32[8,1,256]{2,1,0:T(1,128)S(1)} all-to-all(f32[8,1,256]{2,1,0:T(1,128)S(1)} %broadcast_in_dim.40), channel_id=1, replica_groups=mesh['rep'=2,'fs'=32,'tp'=8] {'tp'}, dimensions={0} | all-to-all | bytes 16384 | tf_op jit(solution)/shard_map/all_to_all | solution.py:23
  529.0 5.8 all-to-all-start.7
  535.1 26.4 %all-to-all-done.7 = bf16[32,64,128]{2,1,0:T(8,128)(2,1)S(1)} async-done(((bf16[32,64,128]{2,1,0:T(8,128)(2,1)}), bf16[32,64,128]{2,1,0:T(8,128)(2,1)S(1)}, u32[]{:S(2)}, u32[]{:S(2)}) %all-to-all-start.7) | async-done | bytes 524320 | tf_op jit(solution)/shard_map/all_to_all | solution.py:23
  561.6 21.2 %all_to_all.76 = bf16[8,256,256]{1,2,0:T(8,128)(2,1)S(1)} all-to-all(bf16[8,256,256]{1,2,0:T(8,128)(2,1)S(1)} %broadcast_in_dim.41), channel_id=1, replica_groups=mesh['rep'=2,'fs'=32,'tp'=8] {'tp'}, dimensions={0} | all-to-all | bytes 2097152 | tf_op jit(solution)/shard_map/all_to_all | solution.py:23
  583.7 6.1 all-to-all-start.5
  595.5 20.9 %all-to-all-done.5 = bf16[32,64,128]{2,1,0:T(8,128)(2,1)} async-done(((bf16[32,64,128]{2,1,0:T(8,128)(2,1)}), bf16[32,64,128]{2,1,0:T(8,128)(2,1)}, u32[]{:S(2)}, u32[]{:S(2)}) %all-to-all-start.5) | async-done | bytes 524320 | tf_op jit(solution)/shard_map/all_to_all | solution.py:23
  618.3 21.2 %all_to_all.77 = bf16[8,256,256]{2,1,0:T(8,128)(2,1)S(1)} all-to-all(bf16[8,256,256]{2,1,0:T(8,128)(2,1)S(1)} %bitcast.79), channel_id=1, replica_groups=mesh['rep'=2,'fs'=32,'tp'=8] {'tp'}, dimensions={0} | all-to-all | bytes 2097152 | tf_op jit(solution)/shard_map/all_to_all | solution.py:38
  640.4 4.3 all-to-all-start.10
  644.7 4.6 all-to-all-done.10
  649.6 18.1 %all_to_all.78 = bf16[8,256,256]{1,2,0:T(8,128)(2,1)S(1)} all-to-all(bf16[8,256,256]{1,2,0:T(8,128)(2,1)S(1)} %broadcast_in_dim.47), channel_id=1, replica_groups=mesh['rep'=2,'fs'=32,'tp'=8] {'tp'}, dimensions={0} | all-to-all | bytes 2097152 | tf_op jit(solution)/shard_map/all_to_all | solution.py:23
  668.4 3.2 fusion.8
  671.6 7.4 %fusion.15 = bf16[256,2048]{1,0:T(8,128)(2,1)S(1)} fusion(bf16[2048,2112]{1,0:T(8,128)(2,1)} %bitcast.76, bf16[256,2048]{0,1:T(8,128)(2,1)S(1)} %fusion.22, f32[256,704]{0,1:T(8,128)S(1)} %fusion.8), kind=kOutput, calls=%fused_computation.16 | convolution fusion | flops 1478000640 | bytes 9109504 | tf_op jit(solution)/shard_map/dot_general | solution.py:93
  679.0 18.4 %all_to_all.79 = bf16[8,256,256]{2,1,0:T(8,128)(2,1)S(1)} all-to-all(bf16[8,256,256]{2,1,0:T(8,128)(2,1)S(1)} %bitcast.80), channel_id=1, replica_groups=mesh['rep'=2,'fs'=32,'tp'=8] {'tp'}, dimensions={0} | all-to-all | bytes 2097152 | tf_op jit(solution)/shard_map/all_to_all | solution.py:38
  698.3 4.3 all-to-all-start.13
  702.6 4.6 all-to-all-done.13
  (77 shorter events, 22.9 us)
Async XLA Ops:
  0.0 12.4 %copy-start.2 = (bf16[64,704]{1,0:T(8,128)(2,1)S(1)}, bf16[64,704]{1,0:T(8,128)(2,1)}, u32[]{:S(2)}) copy-start(bf16[64,704]{1,0:T(8,128)(2,1)} %param.12) | copy-start | bytes 270340
  0.0 12.4 %copy-start.3 = (bf16[64,704]{1,0:T(8,128)(2,1)S(1)}, bf16[64,704]{1,0:T(8,128)(2,1)}, u32[]{:S(2)}) copy-start(bf16[64,704]{1,0:T(8,128)(2,1)} %param.13) | copy-start | bytes 270340
  0.0 12.4 %copy-start.4 = (bf16[704,64]{0,1:T(8,128)(2,1)S(1)}, bf16[704,64]{0,1:T(8,128)(2,1)}, u32[]{:S(2)}) copy-start(bf16[704,64]{0,1:T(8,128)(2,1)} %param.14) | copy-start | bytes 270340
  2.1 25.3 %all-to-all-start = ((bf16[8,256,256]{1,2,0:T(8,128)(2,1)}), bf16[8,256,256]{1,2,0:T(8,128)(2,1)S(1)}, u32[]{:S(2)}, u32[]{:S(2)}) async-start(bf16[8,256,256]{1,2,0:T(8,128)(2,1)} %broadcast_in_dim.39), calls=%async_computation | async-start | bytes 2097152 | tf_op jit(solution)/shard_map/all_to_all | solution.py:23
  28.6 399.0 %copy-start.6 = (bf16[128,64]{0,1:T(8,128)(2,1)S(1)}, bf16[128,64]{0,1:T(8,128)(2,1)}, u32[]{:S(2)}) copy-start(bf16[128,64]{0,1:T(8,128)(2,1)} %param.19) | copy-start | bytes 49156
  28.6 407.0 %copy-start.5 = (f32[6,2048]{1,0:T(8,128)S(1)}, f32[6,2048]{1,0:T(8,128)}, u32[]{:S(2)}) copy-start(f32[6,2048]{1,0:T(8,128)} %param.11) | copy-start | bytes 147460
  428.6 33.7 %all-to-all-start.8 = ((bf16[32,128,64]{1,2,0:T(8,128)(2,1)}), bf16[32,128,64]{1,2,0:T(8,128)(2,1)S(1)}, u32[]{:S(2)}, u32[]{:S(2)}) async-start(bf16[32,128,64]{1,2,0:T(8,128)(2,1)} %broadcast_in_dim.45), calls=%async_computation.8 | async-start | bytes 1048576 | tf_op jit(solution)/shard_map/all_to_all | solution.py:23
  446.9 36.6 %copy-start.7 = (bf16[64,128]{1,0:T(8,128)(2,1)S(1)}, bf16[64,128]{1,0:T(8,128)(2,1)}, u32[]{:S(2)}) copy-start(bf16[64,128]{1,0:T(8,128)(2,1)} %param.17) | copy-start | bytes 49156
  483.5 44.5 %copy-start.8 = (bf16[64,128]{1,0:T(8,128)(2,1)S(1)}, bf16[64,128]{1,0:T(8,128)(2,1)}, u32[]{:S(2)}) copy-start(bf16[64,128]{1,0:T(8,128)(2,1)} %param.15) | copy-start | bytes 49156
  484.5 50.3 %copy-start.1 = (bf16[256,256]{1,0:T(8,128)(2,1)S(1)}, bf16[256,256]{1,0:T(8,128)(2,1)}, u32[]{:S(2)}) copy-start(bf16[256,256]{1,0:T(8,128)(2,1)} %param.10) | copy-start | bytes 393220
  484.5 32.7 %all-to-all-start.6 = ((bf16[32,64,128]{2,1,0:T(8,128)(2,1)}), bf16[32,64,128]{2,1,0:T(8,128)(2,1)S(1)}, u32[]{:S(2)}, u32[]{:S(2)}) async-start(bf16[32,64,128]{2,1,0:T(8,128)(2,1)} %broadcast_in_dim.43), calls=%async_computation.6 | async-start | bytes 1048576 | tf_op jit(solution)/shard_map/all_to_all | solution.py:23
  517.2 11.7 %copy-start = (bf16[32,64,128]{2,1,0:T(8,128)(2,1)}, bf16[32,64,128]{2,1,0:T(8,128)(2,1)S(1)}, u32[]{:S(2)}) copy-start(bf16[32,64,128]{2,1,0:T(8,128)(2,1)S(1)} %all-to-all-done.6) | copy-start | bytes 1572868
  529.0 32.6 %all-to-all-start.7 = ((bf16[32,64,128]{2,1,0:T(8,128)(2,1)}), bf16[32,64,128]{2,1,0:T(8,128)(2,1)S(1)}, u32[]{:S(2)}, u32[]{:S(2)}) async-start(bf16[32,64,128]{2,1,0:T(8,128)(2,1)} %broadcast_in_dim.44), calls=%async_computation.7 | async-start | bytes 1048576 | tf_op jit(solution)/shard_map/all_to_all | solution.py:23
  534.8 48.0 %copy-start.9 = (bf16[64,128]{1,0:T(8,128)(2,1)S(1)}, bf16[64,128]{1,0:T(8,128)(2,1)}, u32[]{:S(2)}) copy-start(bf16[64,128]{1,0:T(8,128)(2,1)} %param.16) | copy-start | bytes 49156
  583.7 32.7 %all-to-all-start.5 = ((bf16[32,64,128]{2,1,0:T(8,128)(2,1)}), bf16[32,64,128]{2,1,0:T(8,128)(2,1)}, u32[]{:S(2)}, u32[]{:S(2)}) async-start(bf16[32,64,128]{2,1,0:T(8,128)(2,1)} %broadcast_in_dim.42), calls=%async_computation.5 | async-start | bytes 1048576 | tf_op jit(solution)/shard_map/all_to_all | solution.py:23
  590.5 4.9 copy-start.10
  592.5 23.8 %collective-permute-start = (f32[2,128]{1,0:T(2,128)S(1)}, f32[2,128]{1,0:T(2,128)S(1)}, u32[]{:S(2)}, u32[]{:S(2)}) collective-permute-start(f32[2,128]{1,0:T(2,128)S(1)} %slice.63), channel_id=1, source_target_pairs={{0,8},{8,16},{16,24},{24,32},{32,40},{40,48},{48,56},{56,64},{64,7... | collective-permute-start | bytes 3080 | tf_op jit(solution)/shard_map/ppermute | solution.py:61
  640.4 8.9 %all-to-all-start.10 = ((f32[8,1,256]{2,1,0:T(1,128)}), f32[8,1,256]{2,1,0:T(1,128)S(1)}, u32[]{:S(2)}, u32[]{:S(2)}) async-start(f32[8,1,256]{2,1,0:T(1,128)} %broadcast_in_dim.46), calls=%async_computation.10 | async-start | bytes 16384 | tf_op jit(solution)/shard_map/all_to_all | solution.py:23
  698.3 8.9 %all-to-all-start.13 = ((f32[8,1,256]{2,1,0:T(1,128)}), f32[8,1,256]{2,1,0:T(1,128)S(1)}, u32[]{:S(2)}, u32[]{:S(2)}) async-start(f32[8,1,256]{2,1,0:T(1,128)} %broadcast_in_dim.48), calls=%async_computation.13 | async-start | bytes 16384 | tf_op jit(solution)/shard_map/all_to_all | solution.py:23
